TPU v7x, 512 devices: a whole 4x4x16 slice. The times are simulated.
512 devices in a mesh: sp: 64 (over z, y), tp: 8 (over x, core).
Axes of the slice: x: 4, y: 4, z: 16, core: 2. Of those that a mesh axis runs over, the one named last changes fastest.
Arguments:
- queries: bfloat16 [16384, 1024], P('sp', 'tp'), may hold values from -6 to 6
- keys: bfloat16 [16384, 512], P('sp', 'tp'), may hold values from -6 to 6
- values: bfloat16 [16384, 512], P('sp', 'tp'), may hold values from -6 to 6
- q_gain: float32 [64], replicated, may hold values from 1.6 to 4.5
- key_norm_gain: float32 [64], replicated, may hold values from 1.6 to 4.5
- out_weight: bfloat16 [1024, 2048], P('tp'), may hold values from -0.1875 to 0.1875
- residual: bfloat16 [16384, 2048], P('sp'), may hold values from -6 to 6
- ln1_gain: float32 [2048], replicated, may hold values from 0.1 to 1.9
- ln1_bias: float32 [2048], replicated, may hold values from -3 to 3
- up_weight: bfloat16 [2048, 8192], P('sp', 'tp'), may hold values from -0.125 to 0.125
- down_weight: bfloat16 [8192, 2048], P('tp', 'sp'), may hold values from -0.0625 to 0.0625
- ln2_gain: float32 [2048], replicated, may hold values from 0.1 to 1.9
- ln2_bias: float32 [2048], replicated, may hold values from -3 to 3
Outputs:
- encoded: bfloat16 [16384, 2048], P('sp', 'tp')
All inputs are finite; a program needn't handle non-finite values.
Results may differ from a plain program's by a relative error of at most 0.014.
Values may be sent and summed in bfloat16 or wider, within the bound.
A program may use at most 64 MiB of HBM per device.

v0:
```python
import math
import jax
import jax.numpy as jnp
from jax import lax
from jax.sharding import PartitionSpec as P

D = 2048
HEAD_SIZE = 64
GRID_W = 64
ALPHA = 8.0**0.25
ROTARY_BASE = 10000.0
RMS_EPSILON = 1e-06
NORM_EPSILON = 1e-05


def turned_gather(arrays, axis, dims):
    turned = [jnp.moveaxis(a, dim, 0) for a, dim in zip(arrays, dims)]
    both = jnp.concatenate([t.reshape(len(t), -1) for t in turned], axis=1)
    out, at, finished = (lax.all_gather(both, axis, axis=0, tiled=True), 0, [])
    for t, dim in zip(turned, dims):
        piece = out[:, at : at + t[0].size].reshape(-1, *t.shape[1:])
        finished.append(jnp.moveaxis(piece, 0, dim))
        at += t[0].size
    return tuple(finished)


def side_by_side(arrays, axis, dim, along):
    widths = [a.shape[along] for a in arrays]
    both = jnp.concatenate(arrays, axis=along)
    out = lax.all_gather(both, axis, axis=dim, tiled=True)
    return tuple(jnp.split(out, [sum(widths[:k]) for k in range(1, len(widths))], axis=along))


def split_up(array, dim, devices):
    before, after = (array.shape[:dim], array.shape[dim + 1 :])
    return jnp.moveaxis(array.reshape(*before, devices, -1, *after), dim, 0)


def sent_and_summed(array, axis, dim):
    devices = lax.axis_size(axis)
    blocks = lax.all_to_all(split_up(array, dim, devices), axis, 0, 0, tiled=True)
    return jnp.sum(blocks.astype(jnp.float32), axis=0)


def from_everyone(array, axis):
    devices = lax.axis_size(axis)
    return lax.all_to_all(
        jnp.broadcast_to(array[None], (devices, *array.shape)), axis, 0, 0, tiled=True
    )


def over_copies(array, axis):
    everything = from_everyone(array, axis)
    return jnp.sum(everything, axis=0)


def in_one(arrays, axis):
    ends = [0]
    for a in arrays:
        ends.append(ends[-1] + a.size)
    running = over_copies(jnp.concatenate([a.ravel() for a in arrays]), axis)
    return tuple((running[b:e].reshape(a.shape) for a, b, e in zip(arrays, ends, ends[1:])))


def laid_out(blocks, dim):
    lengths = list(blocks.shape[1:])
    lengths[dim] *= blocks.shape[0]
    return jnp.moveaxis(blocks, 0, dim).reshape(lengths)


def gathered_copies(array, axis, dim):
    return laid_out(from_everyone(array, axis), dim)


def rotate_grid(heads_in, grid_places):
    half_dim = heads_in.shape[-1] // 2
    quarter = half_dim // 2
    inverse = ROTARY_BASE ** (-jnp.arange(quarter, dtype=jnp.float32) / quarter)

    def spin(segment, coords):
        angles = coords.astype(jnp.float32)[:, None] * inverse[None, :]
        cos_val = jnp.cos(angles)[:, None, :]
        sin_val = jnp.sin(angles)[:, None, :]
        lead_half = segment[..., :quarter]
        tail_half = segment[..., quarter:]
        return jnp.concatenate(
            [lead_half * cos_val - tail_half * sin_val, tail_half * cos_val + lead_half * sin_val],
            -1,
        )

    return jnp.concatenate(
        [
            spin(heads_in[..., :half_dim], grid_places // GRID_W),
            spin(heads_in[..., half_dim:], grid_places % GRID_W),
        ],
        -1,
    )


def prepare_inputs(heads_in, gain_vec, grid_places, factor):
    values32 = heads_in.astype(jnp.float32)
    normed = (
        values32
        * lax.rsqrt(jnp.mean(values32 * values32, -1, keepdims=True) + RMS_EPSILON)
        * gain_vec
    )
    return (rotate_grid(normed, grid_places) * factor).astype(jnp.bfloat16)


def finish_norm(pre_norm, stats, gain_vec, bias_vec):
    row_mean = stats[0][:, None] / D
    spread = stats[1][:, None] / D - row_mean * row_mean
    return (pre_norm - row_mean) * lax.rsqrt(spread + NORM_EPSILON) * gain_vec + bias_vec


def take_cols(array_in, col_start, col_width):
    return lax.dynamic_slice_in_dim(array_in, col_start, col_width, array_in.ndim - 1)


def local(
    queries,
    keys,
    values,
    q_gain,
    key_norm_gain,
    out_weight,
    residual,
    ln1_gain,
    ln1_bias,
    up_weight,
    down_weight,
    ln2_gain,
    ln2_bias,
):
    tok_rows = queries.shape[0]
    up_whole, down_whole = turned_gather((up_weight, down_weight), "sp", (0, 1))
    grid_places = lax.axis_index("sp") * tok_rows + jnp.arange(tok_rows, dtype=jnp.int32)
    kv_heads = keys.shape[1] // HEAD_SIZE
    q_count = queries.shape[1] // HEAD_SIZE
    group_count_size = q_count // kv_heads
    query_head_rows = prepare_inputs(
        queries.reshape(tok_rows, q_count, HEAD_SIZE), q_gain, grid_places, HEAD_SIZE ** (-0.5)
    )
    q_grouped = query_head_rows.reshape(tok_rows, kv_heads, group_count_size, HEAD_SIZE)
    k_sent = prepare_inputs(
        keys.reshape(tok_rows, kv_heads, HEAD_SIZE), key_norm_gain, grid_places, 1.0
    ).reshape(tok_rows, kv_heads * HEAD_SIZE)
    initial = (
        jnp.full((kv_heads, group_count_size, tok_rows), -jnp.inf, jnp.float32),
        jnp.zeros((kv_heads, group_count_size, tok_rows), jnp.float32),
        jnp.zeros((tok_rows, kv_heads, group_count_size, HEAD_SIZE), jnp.float32),
    )
    key_piece, value_piece = side_by_side((k_sent, values), "sp", 0, 1)
    key_count = key_piece.shape[0]
    block_len = math.gcd(key_count, 2048)
    key_blocks = key_piece.reshape(key_count // block_len, block_len, kv_heads, HEAD_SIZE)
    value_blocks = value_piece.reshape(key_count // block_len, block_len, kv_heads, HEAD_SIZE)

    def advance(state_in, blocks):
        maxima, totals, accumulated = state_in
        scores = jnp.einsum(
            "qhgd,khd->hgqk", q_grouped, blocks[0], preferred_element_type=jnp.float32
        )
        new_max = jnp.maximum(maxima, jnp.max(scores, -1))
        factor = jnp.exp(maxima - new_max)
        weights = jnp.exp(scores - new_max[..., None])
        totals = totals * factor + jnp.sum(weights, -1)
        update = jnp.einsum(
            "hgqk,khd->qhgd",
            weights.astype(jnp.bfloat16),
            blocks[1],
            preferred_element_type=jnp.float32,
        )
        accumulated = accumulated * jnp.transpose(factor, (2, 0, 1))[..., None] + update
        return ((new_max, totals, accumulated), None)

    state_out, unused = lax.scan(advance, initial, (key_blocks, value_blocks))
    maxima, totals, accumulated = state_out
    attended = (
        (accumulated / jnp.transpose(totals, (2, 0, 1))[..., None])
        .reshape(tok_rows, q_count * HEAD_SIZE)
        .astype(jnp.bfloat16)
    )
    partial_value = jnp.dot(attended, out_weight, preferred_element_type=jnp.float32)
    col_width = D // lax.axis_size("tp")
    col_start = lax.axis_index("tp") * col_width
    mixed_cols = sent_and_summed(partial_value.astype(jnp.bfloat16), "tp", 1)
    pre_norm = ALPHA * take_cols(residual, col_start, col_width).astype(jnp.float32) + mixed_cols
    stats = in_one((jnp.sum(pre_norm, -1), jnp.sum(pre_norm * pre_norm, -1)), "tp")
    normed_own = finish_norm(
        pre_norm,
        stats,
        take_cols(ln1_gain, col_start, col_width),
        take_cols(ln1_bias, col_start, col_width),
    ).astype(jnp.bfloat16)
    full_rows = gathered_copies(normed_own, "tp", 1)
    up_acts = jnp.dot(full_rows, up_whole, preferred_element_type=jnp.float32)
    hidden = jnp.square(jnp.maximum(up_acts, 0.0)).astype(jnp.bfloat16)
    partial_ffn = jnp.dot(hidden, down_whole, preferred_element_type=jnp.float32)
    ffn_cols = sent_and_summed(partial_ffn.astype(jnp.bfloat16), "tp", 1)
    second = ALPHA * normed_own.astype(jnp.float32) + ffn_cols
    stats_two = in_one((jnp.sum(second, -1), jnp.sum(second * second, -1)), "tp")
    return finish_norm(
        second,
        stats_two,
        take_cols(ln2_gain, col_start, col_width),
        take_cols(ln2_bias, col_start, col_width),
    ).astype(jnp.bfloat16)


def solution(mesh):
    return jax.shard_map(
        local,
        mesh=mesh,
        in_specs=(
            P("sp", "tp"),
            P("sp", "tp"),
            P("sp", "tp"),
            P(),
            P(),
            P("tp", None),
            P("sp", None),
            P(),
            P(),
            P("sp", "tp"),
            P("tp", "sp"),
            P(),
            P(),
        ),
        out_specs=P("sp", "tp"),
        check_vma=False,
    )
```

profile of v0, /device:TPU:1, one launch (start us, length us, event | category | flops | bytes accessed | tf_op | source)
XLA Modules:
  0.0 357.5 jit_solution(9664578682468562471)
XLA Ops:
  10.3 1.5 pad_maximum_fusion
  13.9 137.4 %all-gather.3.cloned.1.call-done = bf16[16384,128]{0,1:T(8,128)(2,1)} async-done(((bf16[256,128]{0,1:T(8,128)(2,1)}), bf16[16384,128]{0,1:T(8,128)(2,1)}) %all-gather.3.cloned.1.call-update) | async-done | bytes 4194320 | tf_op jit(solution)/shard_map/all_gather | solution.py:30
  151.3 2.6 fusion.67
  153.9 1.2 copy.53
  157.4 2.5 copy.38
  159.9 54.9 %while.15 = (s32[]{:T(128)}, f32[1,2,256]{2,1,0:T(2,128)S(1)}, f32[1,2,256]{2,1,0:T(2,128)S(1)}, f32[256,1,2,64]{0,3,2,1:T(8,128)S(1)}, bf16[8,2048,1,64]{1,3,2,...) while((s32[]{:T(128)}, f32[1,2,256]{2,1,0:T(2,128)S(1)}, ...), condition=%wide.region_5.6_spmd.clone, body=%wide.region_2.5_spmd.clone.sunk | while | flops 273779712 | bytes 30245512 | solution.py:177
  159.9 2.7 bitcast_reduce_fusion.2
  162.7 3.2 fusion.80
  166.8 2.7 bitcast_reduce_fusion.2
  169.5 3.2 fusion.80
  173.6 2.7 bitcast_reduce_fusion.2
  176.4 3.2 fusion.80
  180.5 2.7 bitcast_reduce_fusion.2
  183.2 3.2 fusion.80
  187.4 2.7 bitcast_reduce_fusion.2
  190.1 3.2 fusion.80
  194.2 2.7 bitcast_reduce_fusion.2
  197.0 3.2 fusion.80
  201.1 2.7 bitcast_reduce_fusion.2
  203.9 3.2 fusion.80
  208.0 2.7 bitcast_reduce_fusion.2
  210.7 3.2 fusion.80
  216.5 14.5 %all-to-all-start = ((bf16[8,256,256]{2,1,0:T(8,128)(2,1)}), bf16[8,256,256]{2,1,0:T(8,128)(2,1)S(1)}, u32[]{:S(2)}, u32[]{:S(2)}) async-start(bf16[8,256,256]{2,1,0:T(8,128)(2,1)} %bitcast.113), calls=%async_computation | async-start | bytes 2097152 | tf_op jit(solution)/shard_map/all_to_all | solution.py:41
  231.0 15.0 %all-to-all-done = bf16[8,256,256]{2,1,0:T(8,128)(2,1)S(1)} async-done(((bf16[8,256,256]{2,1,0:T(8,128)(2,1)}), bf16[8,256,256]{2,1,0:T(8,128)(2,1)S(1)}, u32[]{:S(2)}, u32[]{:S(2)}) %all-to-all-start) | async-done | bytes 1048608 | tf_op jit(solution)/shard_map/all_to_all | solution.py:41
  247.8 4.2 %all-to-all-start.1 = ((f32[8,1,512]{2,1,0:T(1,128)}), f32[8,1,512]{2,1,0:T(1,128)S(1)}, u32[]{:S(2)}, u32[]{:S(2)}) async-start(f32[8,1,512]{2,1,0:T(1,128)} %broadcast_in_dim.15), calls=%async_computation.1 | async-start | bytes 32768 | tf_op jit(solution)/shard_map/all_to_all | solution.py:47
  253.5 3.2 all-to-all-done.1
  258.0 18.0 %all_to_all.27 = bf16[8,256,256]{1,2,0:T(8,128)(2,1)S(1)} all-to-all(bf16[8,256,256]{1,2,0:T(8,128)(2,1)S(1)} %broadcast_in_dim.16), channel_id=1, replica_groups=mesh['sp'=64,'tp'=8] {'tp'}, dimensions={0} | all-to-all | bytes 2097152 | tf_op jit(solution)/shard_map/all_to_all | solution.py:47
  276.1 30.5 %all-gather.5.cloned.1.call-done = bf16[2048,2048]{1,0:T(8,128)(2,1)} async-done(((bf16[32,2048]{1,0:T(8,128)(2,1)}), bf16[2048,2048]{1,0:T(8,128)(2,1)}) %all-gather.5.cloned.1.call-update) | async-done | bytes 8388624 | tf_op jit(solution)/shard_map/all_gather | solution.py:19
  306.6 5.8 %fusion.26 = bf16[256,2048]{1,0:T(8,128)(2,1)S(1)} fusion(bf16[2048,2048]{1,0:T(8,128)(2,1)} %all-gather.5.cloned.1.call-done, bf16[256,2048]{0,1:T(8,128)(2,1)S(1)} %bitcast.144), kind=kOutput, calls=%fused_computation.30 | convolution fusion | flops 2148794368 | bytes 10485760 | tf_op jit(solution)/shard_map/dot_general | solution.py:199
  312.5 27.4 %all_to_all.28 = bf16[8,256,256]{2,1,0:T(8,128)(2,1)S(1)} all-to-all(bf16[8,256,256]{2,1,0:T(8,128)(2,1)S(1)} %bitcast.141), channel_id=1, replica_groups=mesh['sp'=64,'tp'=8] {'tp'}, dimensions={0} | all-to-all | bytes 2097152 | tf_op jit(solution)/shard_map/all_to_all | solution.py:41
  340.9 4.3 %all-to-all-start.4 = ((f32[8,1,512]{2,1,0:T(1,128)}), f32[8,1,512]{2,1,0:T(1,128)S(1)}, u32[]{:S(2)}, u32[]{:S(2)}) async-start(f32[8,1,512]{2,1,0:T(1,128)} %broadcast_in_dim.17), calls=%async_computation.4 | async-start | bytes 32768 | tf_op jit(solution)/shard_map/all_to_all | solution.py:47
  346.7 3.2 all-to-all-done.4
  (102 shorter events, 24.8 us)
Async XLA Ops:
  6.5 208.4 %copy-start = (bf16[128,2048]{1,0:T(8,128)(2,1)S(1)}, bf16[128,2048]{1,0:T(8,128)(2,1)}, u32[]{:S(2)}) copy-start(bf16[128,2048]{1,0:T(8,128)(2,1)} %param.20) | copy-start | bytes 1572868
  6.5 144.7 %all-gather.3.cloned.1.call-start = ((), (), s32[]{:S(2)}) async-start(), calls=%async_computation.5 | async-start | bytes 4259840 | tf_op jit(solution)/shard_map/all_gather | solution.py:30
  9.6 0.6 copy-start.2
  10.2 296.4 %all-gather.5.cloned.1.call-start = ((), (), s32[]{:S(2)}) async-start(), calls=%async_computation.6 | async-start | bytes 8519680 | tf_op jit(solution)/shard_map/all_gather | solution.py:19
  162.6 3.5 copy-start.1
  169.5 3.5 copy-start.1
  176.4 3.5 copy-start.1
  183.2 3.6 copy-start.1
  190.1 3.5 copy-start.1
  197.0 3.6 copy-start.1
  203.8 3.5 copy-start.1
  210.7 3.6 copy-start.1
  216.5 29.5 %all-to-all-start = ((bf16[8,256,256]{2,1,0:T(8,128)(2,1)}), bf16[8,256,256]{2,1,0:T(8,128)(2,1)S(1)}, u32[]{:S(2)}, u32[]{:S(2)}) async-start(bf16[8,256,256]{2,1,0:T(8,128)(2,1)} %bitcast.113), calls=%async_computation | async-start | bytes 2097152 | tf_op jit(solution)/shard_map/all_to_all | solution.py:41
  247.8 8.9 %all-to-all-start.1 = ((f32[8,1,512]{2,1,0:T(1,128)}), f32[8,1,512]{2,1,0:T(1,128)S(1)}, u32[]{:S(2)}, u32[]{:S(2)}) async-start(f32[8,1,512]{2,1,0:T(1,128)} %broadcast_in_dim.15), calls=%async_computation.1 | async-start | bytes 32768 | tf_op jit(solution)/shard_map/all_to_all | solution.py:47
  340.9 9.0 %all-to-all-start.4 = ((f32[8,1,512]{2,1,0:T(1,128)}), f32[8,1,512]{2,1,0:T(1,128)S(1)}, u32[]{:S(2)}, u32[]{:S(2)}) async-start(f32[8,1,512]{2,1,0:T(1,128)} %broadcast_in_dim.17), calls=%async_computation.4 | async-start | bytes 32768 | tf_op jit(solution)/shard_map/all_to_all | solution.py:47
Sparse Core Ops, SparseCore 0:
  10.4 140.8 all-gather.2
  154.2 152.3 all-gather.4
where the time goes:
time: 358 us; the launch traced here: 357 us
  waiting for transfers between devices  189 us (53%)
  matrix products  53.7 us (15%)
  blocking collectives  45.5 us (13%)
  starting transfers between devices  23 us (6%)
  local copies, waits for them, and re-layouts  19.1 us (5%)
  between operations  13.6 us (4%)
  other arithmetic  13 us (4%)
    all_gather x1, waiting for transfers between devices, side_by_side(): out = lax.all_gather(both, axis, axis=dim, tiled=True)  137 us
    all_gather x1, waiting for transfers between devices, turned_gather(): out, at, finished = (lax.all_gather(both, axis, axis=0, tiled=True), 0, [])  30.5 us
    all_to_all x1, blocking collectives, sent_and_summed(): lax.all_to_all(split_up(array, dim, devices), axis, 0, 0, tiled=True)  27.4 us
    dot_general x8, matrix products, advance(): jnp.einsum('hgqk,khd->qhgd', weights.astype(jnp.bfloat16), blocks[1], pre...  25.7 us
    dot_general x8, matrix products, advance(): jnp.einsum('qhgd,khd->hgqk', q_grouped, blocks[0], preferred_element_type...  21.7 us
    all_to_all x1, blocking collectives, from_everyone(): lax.all_to_all(jnp.broadcast_to(array[None], (devices, *array.shape)), ax...  18 us
    all_to_all x1, waiting for transfers between devices, sent_and_summed(): lax.all_to_all(split_up(array, dim, devices), axis, 0, 0, tiled=True)  15 us
    all_to_all x1, starting transfers between devices, sent_and_summed(): lax.all_to_all(split_up(array, dim, devices), axis, 0, 0, tiled=True)  14.5 us
  transfers between devices with their start and end apart: 5, of which 5 were waited for; matrix products, arithmetic and copies ran while one was open for 20% of the time, Pallas kernels for 0%

commit v1 on v0

--- a/solution.py
+++ b/solution.py
@@ -16,7 +16,13 @@
 def turned_gather(arrays, axis, dims):
     turned = [jnp.moveaxis(a, dim, 0) for a, dim in zip(arrays, dims)]
     both = jnp.concatenate([t.reshape(len(t), -1) for t in turned], axis=1)
-    out, at, finished = (lax.all_gather(both, axis, axis=0, tiled=True), 0, [])
+    out, at, finished = (
+        jnp.concatenate(
+            lax.all_to_all(jnp.stack([both] * lax.axis_size(axis)), axis, 0, 0), axis=0
+        ),
+        0,
+        [],
+    )
     for t, dim in zip(turned, dims):
         piece = out[:, at : at + t[0].size].reshape(-1, *t.shape[1:])
         finished.append(jnp.moveaxis(piece, 0, dim))

time: 358 us -> 708 us (1.98)
  blocking collectives: 45.5 us -> 397 us
  other arithmetic: 13 us -> 30.2 us
  waiting for transfers between devices: 189 us -> 175 us
  matrix products: 53.7 us -> 41.5 us
    all_to_all x1, blocking collectives: 18 us -> 373 us  [turned_gather(): lax.all_to_all(jnp.stack([both] * lax.axis_size(axis)), axis, 0, 0)]
    all_gather x1 -> x0, waiting for transfers between devices: 30.5 us -> none  [turned_gather(): out, at, finished = (lax.all_gather(both, axis, axis=0, tiled=True), 0, [])]
    reduce_sum x8, other arithmetic: 4.52 us -> 23.2 us  [advance(): totals = totals * factor + jnp.sum(weights, -1)]
    all_to_all x2 -> x3, waiting for transfers between devices: 6.38 us -> 21.3 us  [from_everyone(): lax.all_to_all(jnp.broadcast_to(array[None], (devices, *array.shape)), ax...]
    dot_general x8, matrix products: 25.7 us -> 13.9 us  [advance(): jnp.einsum('hgqk,khd->qhgd', weights.astype(jnp.bfloat16), blocks[1], pre...]
  transfers between devices with their start and end apart: 5 -> 5, of which waited for: 5 -> 5; matrix products, arithmetic and copies ran while one was open for 20% -> 1% of each run, Pallas kernels for 0% -> 0%
where the time goes in v1:
time: 708 us; the launch traced here: 707 us
  blocking collectives  397 us (56%)
  waiting for transfers between devices  175 us (25%)
  matrix products  41.5 us (6%)
  other arithmetic  30.2 us (4%)
  starting transfers between devices  27.2 us (4%)
  local copies, waits for them, and re-layouts  22.6 us (3%)
  between operations  13.6 us (2%)
    all_to_all x1, blocking collectives, turned_gather(): lax.all_to_all(jnp.stack([both] * lax.axis_size(axis)), axis, 0, 0)  373 us
    all_gather x1, waiting for transfers between devices, side_by_side(): out = lax.all_gather(both, axis, axis=dim, tiled=True)  139 us
    all_to_all x1, blocking collectives, sent_and_summed(): lax.all_to_all(split_up(array, dim, devices), axis, 0, 0, tiled=True)  23.6 us
    reduce_sum x8, other arithmetic, advance(): totals = totals * factor + jnp.sum(weights, -1)  23.2 us
    dot_general x8, matrix products, advance(): jnp.einsum('qhgd,khd->hgqk', q_grouped, blocks[0], preferred_element_type...  21.3 us
    all_to_all x3, waiting for transfers between devices, from_everyone(): lax.all_to_all(jnp.broadcast_to(array[None], (devices, *array.shape)), ax...  21.3 us
    all_to_all x1, waiting for transfers between devices, sent_and_summed(): lax.all_to_all(split_up(array, dim, devices), axis, 0, 0, tiled=True)  15 us
    all_to_all x1, starting transfers between devices, sent_and_summed(): lax.all_to_all(split_up(array, dim, devices), axis, 0, 0, tiled=True)  14.5 us
  transfers between devices with their start and end apart: 5, of which 5 were waited for; matrix products, arithmetic and copies ran while one was open for 1% of the time, Pallas kernels for 0%

profile of v1, /device:TPU:1, one launch (start us, length us, event | category | flops | bytes accessed | tf_op | source)
XLA Modules:
  0.0 707.3 jit_solution(16376542717463174036)
XLA Ops:
  12.3 139.0 %all-gather.2.cloned.1.call-done = bf16[16384,128]{0,1:T(8,128)(2,1)} async-done(((bf16[256,128]{0,1:T(8,128)(2,1)}), bf16[16384,128]{0,1:T(8,128)(2,1)}) %all-gather.2.cloned.1.call-update) | async-done | bytes 4194320 | tf_op jit(solution)/shard_map/all_gather | solution.py:36
  151.3 2.6 fusion.67
  157.4 2.5 copy.38
  159.9 63.0 %while.15 = (s32[]{:T(128)}, f32[1,2,256]{2,1,0:T(2,128)S(1)}, f32[1,2,256]{2,1,0:T(2,128)S(1)}, f32[256,1,2,64]{0,3,2,1:T(8,128)S(1)}, bf16[8,2048,1,64]{1,3,2,...) while((s32[]{:T(128)}, f32[1,2,256]{2,1,0:T(2,128)S(1)}, ...), condition=%wide.region_5.6_spmd.clone, body=%wide.region_2.5_spmd.clone.sunk | while | flops 273779712 | bytes 30245012 | solution.py:183
  159.9 2.7 bitcast_reduce_fusion.2
  162.6 2.9 fusion.79
  167.8 2.7 bitcast_reduce_fusion.2
  170.5 2.9 fusion.79
  173.9 1.7 fusion.80
  175.7 2.7 bitcast_reduce_fusion.2
  178.4 2.9 fusion.79
  183.6 2.7 bitcast_reduce_fusion.2
  186.2 2.9 fusion.79
  191.4 2.7 bitcast_reduce_fusion.2
  194.1 2.9 fusion.79
  199.3 2.7 bitcast_reduce_fusion.2
  202.0 2.9 fusion.79
  207.2 2.7 bitcast_reduce_fusion.2
  209.9 2.9 fusion.79
  215.0 2.7 bitcast_reduce_fusion.2
  217.7 2.9 fusion.79
  224.5 14.5 %all-to-all-start = ((bf16[8,256,256]{2,1,0:T(8,128)(2,1)}), bf16[8,256,256]{2,1,0:T(8,128)(2,1)S(1)}, u32[]{:S(2)}, u32[]{:S(2)}) async-start(bf16[8,256,256]{2,1,0:T(8,128)(2,1)} %bitcast.114), calls=%async_computation | async-start | bytes 2097152 | tf_op jit(solution)/shard_map/all_to_all | solution.py:47
  239.0 15.0 %all-to-all-done = bf16[8,256,256]{2,1,0:T(8,128)(2,1)S(1)} async-done(((bf16[8,256,256]{2,1,0:T(8,128)(2,1)}), bf16[8,256,256]{2,1,0:T(8,128)(2,1)S(1)}, u32[]{:S(2)}, u32[]{:S(2)}) %all-to-all-start) | async-done | bytes 1048608 | tf_op jit(solution)/shard_map/all_to_all | solution.py:47
  255.8 4.2 all-to-all-start.1
  261.5 3.2 all-to-all-done.1
  266.9 4.2 all-to-all-start.2
  271.1 15.0 %all-to-all-done.2 = bf16[8,256,256]{1,2,0:T(8,128)(2,1)S(1)} async-done(((bf16[8,256,256]{1,2,0:T(8,128)(2,1)}), bf16[8,256,256]{1,2,0:T(8,128)(2,1)S(1)}, u32[]{:S(2)}, u32[]{:S(2)}) %all-to-all-start.2) | async-done | bytes 1048608 | tf_op jit(solution)/shard_map/all_to_all | solution.py:53
  287.2 373.1 %all_to_all.32 = bf16[64,32,2048]{2,1,0:T(8,128)(2,1)} all-to-all(bf16[64,32,2048]{2,1,0:T(8,128)(2,1)S(1)} %stack.2), channel_id=1, replica_groups=mesh['sp'=64,'tp'=8] {'sp'}, dimensions={0} | all-to-all | bytes 16777216 | tf_op jit(solution)/shard_map/all_to_all | solution.py:21
  660.2 5.8 fusion.26
  666.1 23.6 %all_to_all.33 = bf16[8,256,256]{2,1,0:T(8,128)(2,1)S(1)} all-to-all(bf16[8,256,256]{2,1,0:T(8,128)(2,1)S(1)} %bitcast.143), channel_id=1, replica_groups=mesh['sp'=64,'tp'=8] {'tp'}, dimensions={0} | all-to-all | bytes 2097152 | tf_op jit(solution)/shard_map/all_to_all | solution.py:47
  690.7 4.3 all-to-all-start.5
  696.5 3.2 all-to-all-done.5
  (106 shorter events, 37.1 us)
Async XLA Ops:
  6.5 216.4 %copy-start = (bf16[128,2048]{1,0:T(8,128)(2,1)S(1)}, bf16[128,2048]{1,0:T(8,128)(2,1)}, u32[]{:S(2)}) copy-start(bf16[128,2048]{1,0:T(8,128)(2,1)} %param.20) | copy-start | bytes 1572868
  6.5 144.8 %all-gather.2.cloned.1.call-start = ((), (), s32[]{:S(2)}) async-start(), calls=%async_computation.6 | async-start | bytes 4259840 | tf_op jit(solution)/shard_map/all_gather | solution.py:36
  9.6 0.6 copy-start.2
  162.6 3.4 copy-start.1
  170.5 3.4 copy-start.1
  178.3 3.4 copy-start.1
  186.2 3.4 copy-start.1
  194.1 3.4 copy-start.1
  202.0 3.4 copy-start.1
  209.8 3.4 copy-start.1
  217.7 3.4 copy-start.1
  224.5 46.7 %copy-start.3 = (bf16[1024,32]{0,1:T(8,128)(2,1)S(1)}, bf16[1024,32]{0,1:T(8,128)(2,1)}, u32[]{:S(2)}) copy-start(bf16[1024,32]{0,1:T(8,128)(2,1)} %param.25) | copy-start | bytes 196612
  224.5 46.7 %copy-start.4 = (bf16[32,1024]{1,0:T(8,128)(2,1)S(1)}, bf16[32,1024]{1,0:T(8,128)(2,1)}, u32[]{:S(2)}) copy-start(bf16[32,1024]{1,0:T(8,128)(2,1)} %param.24) | copy-start | bytes 196612
  224.5 29.5 %all-to-all-start = ((bf16[8,256,256]{2,1,0:T(8,128)(2,1)}), bf16[8,256,256]{2,1,0:T(8,128)(2,1)S(1)}, u32[]{:S(2)}, u32[]{:S(2)}) async-start(bf16[8,256,256]{2,1,0:T(8,128)(2,1)} %bitcast.114), calls=%async_computation | async-start | bytes 2097152 | tf_op jit(solution)/shard_map/all_to_all | solution.py:47
  255.8 8.9 %all-to-all-start.1 = ((f32[8,1,512]{2,1,0:T(1,128)}), f32[8,1,512]{2,1,0:T(1,128)S(1)}, u32[]{:S(2)}, u32[]{:S(2)}) async-start(f32[8,1,512]{2,1,0:T(1,128)} %broadcast_in_dim.15), calls=%async_computation.1 | async-start | bytes 32768 | tf_op jit(solution)/shard_map/all_to_all | solution.py:53
  266.9 19.2 %all-to-all-start.2 = ((bf16[8,256,256]{1,2,0:T(8,128)(2,1)}), bf16[8,256,256]{1,2,0:T(8,128)(2,1)S(1)}, u32[]{:S(2)}, u32[]{:S(2)}) async-start(bf16[8,256,256]{1,2,0:T(8,128)(2,1)} %broadcast_in_dim.16), calls=%async_computation.2 | async-start | bytes 2097152 | tf_op jit(solution)/shard_map/all_to_all | solution.py:53
  690.7 9.0 %all-to-all-start.5 = ((f32[8,1,512]{2,1,0:T(1,128)}), f32[8,1,512]{2,1,0:T(1,128)S(1)}, u32[]{:S(2)}, u32[]{:S(2)}) async-start(f32[8,1,512]{2,1,0:T(1,128)} %broadcast_in_dim.17), calls=%async_computation.5 | async-start | bytes 32768 | tf_op jit(solution)/shard_map/all_to_all | solution.py:53
Sparse Core Ops, SparseCore 0:
  10.4 140.8 all-gather.1
